TPU v7x, 32 devices: a whole 2x2x4 slice. The times are simulated.
32 devices in a mesh: ep: 8 (over z, y), tp: 4 (over x, core).
Axes of the slice: x: 2, y: 2, z: 4, core: 2. Of those that a mesh axis runs over, the one named last changes fastest.
Arguments:
- query_rows: bfloat16 [2048, 2048], P('ep', 'tp'), may hold values from -6 to 6
- key_rows: bfloat16 [2048, 512], P('ep', 'tp'), may hold values from -18 to 18
- value_rows: bfloat16 [2048, 512], P('ep', 'tp'), may hold values from -12 to 12
- key_bias: bfloat16 [2048, 8], P('ep', 'tp'), may hold values from -2 to 13
- head_offset: float32 [32], P('tp'), may hold values from -16 to -3
- out_weight: bfloat16 [2048, 2048], P('tp'), may hold values from -0.125 to 0.125
- expert_input: bfloat16 [4096, 2048], P(('ep', 'tp')), may hold values from -40 to 40
- expert_gain: float32 [2048], replicated, may hold values from 0.1 to 1.9
- routes: int32 [4096, 2], P(('ep', 'tp')), may hold values from 0 to 7, all different within a row; in each aligned block of 128 rows (0 to 127, 128 to 255, ...) at most 48 rows name the same one
- route_weight: float32 [4096, 2], P(('ep', 'tp')), may hold values from 0.5 to 2
- gate_weight: bfloat16 [8, 2048, 3584], P('ep', None, 'tp'), may hold values from -0.125 to 0.125
- up_weight: bfloat16 [8, 2048, 3584], P('ep', None, 'tp'), may hold values from -0.125 to 0.125
- down_weight: bfloat16 [8, 3584, 2048], P('ep', 'tp'), may hold values from -0.09375 to 0.09375
Outputs:
- mixed_a: bfloat16 [2048, 2048], P(('ep', 'tp'))
- mixed_b: bfloat16 [4096, 2048], P(('ep', 'tp'))
Inputs may be any that keep to these rules, and one draw needn't show every extreme that they name: `routes`: each row names 2 different experts; in the rows of one device (aligned blocks of 128 rows) no expert is named more than 48 times, and in every draw some device names some expert exactly 48 times.
All inputs are finite; a program needn't handle non-finite values.
Results may differ from a plain program's by a relative error of at most 0.012.
Values may be sent and summed in bfloat16 or wider, within the bound.
A program may use at most 128 MiB of HBM per device.

v0:
```python
import functools
import math

import jax
import jax.numpy as jnp
from jax import lax
from jax.experimental import pallas as pl
from jax.experimental.pallas import tpu as pltpu
from jax.sharding import PartitionSpec as P

HD = 64


EPSILON = 1e-06
CHUNKS = 2


def rms_normed(rows, gain):
    values = rows.astype(jnp.float32)
    scaled = values * lax.rsqrt(jnp.mean(values * values, axis=-1, keepdims=True) + EPSILON)
    return (scaled * gain).astype(jnp.bfloat16)


def stick_kernel(q_ref, kv_ref, tri_ref, out_ref, acc_ref, carry_ref, *, kv_local, group_size):
    block = out_ref.shape[0]
    wide = 2 * HD
    me = lax.axis_index("ep")
    acc_ref[...] = jnp.zeros_like(acc_ref)
    carry_ref[...] = jnp.zeros_like(carry_ref)
    value_width = kv_local * HD

    def tile(index, keep):
        first = pl.multiple_of(index * block, block)
        values = kv_ref[pl.ds(first, block), kv_local * wide : kv_local * wide + value_width]
        for kv in range(kv_local):
            keys = kv_ref[pl.ds(first, block), kv * wide : (kv + 1) * wide]
            for head in range(kv * group_size, (kv + 1) * group_size):
                rows = slice(head * block, (head + 1) * block)
                scores = lax.dot_general(
                    q_ref[rows, :], keys, (((1,), (1,)), ((), ())),
                    preferred_element_type=jnp.float32,
                )
                leave = jnp.maximum(scores, 0.0) + jnp.log(1.0 + jnp.exp(-jnp.abs(scores)))
                log_take = scores - leave
                if keep is not None:
                    leave = jnp.where(keep, leave, 0.0)
                high = leave.astype(jnp.bfloat16)
                low = (leave - high.astype(jnp.float32)).astype(jnp.bfloat16)
                after = jnp.dot(high, tri_ref[...], preferred_element_type=jnp.float32) + jnp.dot(
                    low, tri_ref[...], preferred_element_type=jnp.float32
                )
                carry = carry_ref[rows, :]
                weights = jnp.exp(log_take - after - carry)
                if keep is not None:
                    weights = jnp.where(keep, weights, 0.0)
                acc_ref[rows, :] += jnp.dot(
                    weights.astype(jnp.bfloat16), values, preferred_element_type=jnp.float32
                )
                carry_ref[rows, :] = carry + jnp.broadcast_to(
                    after[:, :1] + leave[:, :1], carry.shape
                )

    query_index = lax.broadcasted_iota(jnp.int32, (block, block), 0)
    key_index = lax.broadcasted_iota(jnp.int32, (block, block), 1)
    tile(me, key_index < query_index)

    def earlier(step, unused):
        tile(me - 1 - step, None)
        return unused

    lax.fori_loop(0, me, earlier, 0)
    for head in range(0, kv_local * group_size):
        kv = head // group_size
        rows = slice(head * block, (head + 1) * block)
        out_ref[:, head * HD : (head + 1) * HD] = acc_ref[rows, kv * HD : (kv + 1) * HD].astype(
            jnp.bfloat16
        )


def gather_keys(key_rows, value_rows, key_bias):
    block = key_rows.shape[0]
    kv_local = key_rows.shape[1] // HD
    wide = 2 * HD
    one = jnp.ones((block, kv_local, 3), jnp.bfloat16)
    key_wide = jnp.concatenate(
        [
            key_rows.reshape(block, kv_local, HD),
            key_bias[:, :, None],
            one,
            jnp.zeros((block, kv_local, wide - HD - 4), jnp.bfloat16),
        ],
        axis=2,
    ).reshape(block, kv_local * wide)
    packed = jnp.concatenate([key_wide, value_rows], axis=1)
    return lax.all_gather(packed, "ep", axis=0, tiled=True)


def stick_heads(query_rows, all_packed, head_offset, kv_local):
    block = query_rows.shape[0]
    heads = query_rows.shape[1] // HD
    group_size = heads // kv_local
    wide = 2 * HD
    first = lax.reduce_precision(head_offset, 8, 7)
    second = lax.reduce_precision(head_offset - first, 8, 7)
    third = head_offset - first - second
    terms = jnp.stack([jnp.ones_like(first), first, second, third], axis=1).astype(jnp.bfloat16)
    queries = jnp.transpose(query_rows.reshape(block, heads, HD), (1, 0, 2)) * jnp.bfloat16(
        1.0 / math.sqrt(HD)
    )
    query_wide = jnp.concatenate(
        [
            queries,
            jnp.broadcast_to(terms[:, None, :], (heads, block, 4)),
            jnp.zeros((heads, block, wide - HD - 4), jnp.bfloat16),
        ],
        axis=2,
    ).reshape(heads * block, wide)
    place = jnp.arange(block)
    tri = (place[:, None] > place[None, :]).astype(jnp.bfloat16)
    span = all_packed.shape[0]
    cells = heads * block * span
    return pl.pallas_call(
        functools.partial(stick_kernel, kv_local=kv_local, group_size=group_size),
        out_shape=jax.ShapeDtypeStruct((block, heads * HD), jnp.bfloat16),
        in_specs=[pl.BlockSpec(memory_space=pltpu.VMEM)] * 3,
        out_specs=pl.BlockSpec(memory_space=pltpu.VMEM),
        scratch_shapes=[
            pltpu.VMEM((heads * block, kv_local * HD), jnp.float32),
            pltpu.VMEM((heads * block, 1), jnp.float32),
        ],
        compiler_params=pltpu.CompilerParams(vmem_limit_bytes=24 * 1024 * 1024),
        cost_estimate=pl.CostEstimate(
            flops=cells * 1000, bytes_accessed=span * 768, transcendentals=cells * 3
        ),
        name="stick",
    )(query_wide, all_packed, tri)


def body(
    query_rows,
    key_rows,
    value_rows,
    key_bias,
    head_offset,
    out_weight,
    expert_input,
    expert_gain,
    routes,
    route_weight,
    gate_weight,
    up_weight,
    down_weight,
):
    kv_local = key_rows.shape[1] // HD
    all_packed = gather_keys(key_rows, value_rows, key_bias)
    normed = rms_normed(expert_input, expert_gain)
    tok_count = normed.shape[0]
    top_count = routes.shape[1]
    model_width = normed.shape[1]
    expert_count = lax.axis_size("ep")
    capacity = max(2, 3 * tok_count * top_count // (2 * expert_count))
    chunks = CHUNKS if capacity % CHUNKS == 0 else 1
    piece = capacity // chunks
    flat_route = routes.reshape(-1)
    one_hot = (flat_route[:, None] == jnp.arange(expert_count)[None, :]).astype(jnp.int32)
    before = jnp.cumsum(one_hot, axis=0) - one_hot
    slot_index = (flat_route * capacity + jnp.sum(before * one_hot, axis=1)).reshape(
        tok_count, top_count
    )
    chunk_rows = expert_count * piece
    hits, arrived = [], []
    for chunk in range(chunks):
        slot_ids = (
            jnp.arange(expert_count)[:, None] * capacity + chunk * piece + jnp.arange(piece)[None, :]
        ).reshape(-1)
        hit = slot_index[None, :, :] == slot_ids[:, None, None]
        hits.append(hit)
        outgoing = jnp.dot(
            jnp.any(hit, axis=2).astype(jnp.bfloat16), normed, preferred_element_type=jnp.float32
        ).astype(jnp.bfloat16)
        outgoing = outgoing.reshape(expert_count, piece, model_width)
        if chunk > 0:
            outgoing, arrived[-1] = lax.optimization_barrier((outgoing, arrived[-1]))
        arrived.append(lax.all_to_all(outgoing, "ep", split_axis=0, concat_axis=0, tiled=True))
    arrived[0], all_packed = lax.optimization_barrier((arrived[0], all_packed))
    results = []
    for chunk in range(chunks):
        row_piece = lax.all_gather(
            arrived[chunk].reshape(chunk_rows, model_width), "tp", axis=0, tiled=True
        )
        gate_act = jnp.dot(row_piece, gate_weight[0], preferred_element_type=jnp.float32)
        up_act = jnp.dot(row_piece, up_weight[0], preferred_element_type=jnp.float32)
        hidden_all = (jax.nn.silu(gate_act) * up_act).astype(jnp.bfloat16)
        partial_sum = jnp.dot(
            hidden_all, down_weight[0], preferred_element_type=jnp.float32
        ).astype(jnp.bfloat16)
        if chunk == chunks - 1:
            partial_sum, query_rows = lax.optimization_barrier((partial_sum, query_rows))
        results.append(
            lax.psum_scatter(partial_sum, "tp", scatter_dimension=0, tiled=True)
        )
    heads_out = stick_heads(query_rows, all_packed, head_offset, kv_local)
    results[0], heads_out = lax.optimization_barrier((results[0], heads_out))
    mixed_a = lax.psum_scatter(
        jnp.dot(heads_out, out_weight, preferred_element_type=jnp.float32).astype(jnp.bfloat16),
        "tp",
        scatter_dimension=0,
        tiled=True,
    )
    total = jnp.zeros((tok_count, model_width), jnp.float32)
    for chunk in range(chunks):
        returned = lax.all_to_all(
            results[chunk].reshape(expert_count, piece, model_width),
            "ep",
            split_axis=0,
            concat_axis=0,
            tiled=True,
        ).reshape(chunk_rows, model_width)
        share = jnp.sum(jnp.where(hits[chunk], route_weight[None, :, :], 0.0), axis=2).T
        for _ in range(3):
            part = lax.reduce_precision(share, 8, 7)
            share = share - part
            total = total + jnp.dot(
                part.astype(jnp.bfloat16), returned, preferred_element_type=jnp.float32
            )
    return (mixed_a, total.astype(jnp.bfloat16))


def solution(mesh):
    return jax.shard_map(
        body,
        mesh=mesh,
        in_specs=(
            P("ep", "tp"),
            P("ep", "tp"),
            P("ep", "tp"),
            P("ep", "tp"),
            P("tp"),
            P("tp", None),
            P(("ep", "tp"), None),
            P(),
            P(("ep", "tp"), None),
            P(("ep", "tp"), None),
            P("ep", None, "tp"),
            P("ep", None, "tp"),
            P("ep", "tp", None),
        ),
        out_specs=(P(("ep", "tp"), None), P(("ep", "tp"), None)),
        check_vma=False,
    )
```

profile of v0, /device:TPU:0, one launch (start us, length us, event | category | flops | bytes accessed | tf_op | source)
XLA Modules:
  0.0 244.5 jit_solution(11018783285823752790)
XLA Ops:
  7.2 0.0 all-gather.4.cloned.1.call-start
  7.2 0.8 copy.56
  8.1 0.9 copy.55
  9.0 0.1 pad.12.clone
  9.1 0.1 pad.11.clone
  9.2 0.1 maximum_maximum_fusion.1
  9.3 0.1 copy.61
  9.4 1.5 pad_maximum_fusion
  11.0 0.8 copy.52
  11.8 0.1 eq.53
  11.9 0.1 eq.49
  12.1 0.6 reduce-window.6
  12.7 0.2 slice_reduce_fusion
  12.9 0.1 iota_add_fusion
  13.0 0.1 fusion.43
  13.1 0.1 reduce_sum.39
  13.2 0.1 copy.54
  13.3 0.1 add.103
  13.4 0.1 iota_add_fusion.1
  13.5 0.1 add.97
  13.5 0.7 multiply_add_fusion
  14.2 0.1 compare_reduce_fusion
  14.4 1.2 fusion.23
  15.6 2.4 convolution_convert_fusion.1
  18.0 7.3 %all-to-all-start = ((bf16[8,24,2048]{2,1,0:T(8,128)(2,1)}), bf16[8,24,2048]{2,1,0:T(8,128)(2,1)S(1)}, u32[]{:S(2)}, u32[]{:S(2)}) async-start(bf16[8,24,2048]{2,1,0:T(8,128)(2,1)} %bitcast.95), calls=%async_computation | async-start | bytes 1572864 | tf_op jit(solution)/shard_map/all_to_all | solution.py:184
  25.3 0.0 all-gather.6.cloned.1.call-start
  25.4 1.3 convolution_convert_fusion.2
  26.7 25.7 %all-to-all-done = bf16[8,24,2048]{2,1,0:T(8,128)(2,1)S(1)} async-done(((bf16[8,24,2048]{2,1,0:T(8,128)(2,1)}), bf16[8,24,2048]{2,1,0:T(8,128)(2,1)S(1)}, u32[]{:S(2)}, u32[]{:S(2)}) %all-to-all-start) | async-done | bytes 786464 | tf_op jit(solution)/shard_map/all_to_all | solution.py:184
  52.5 11.6 %all-gather.4.cloned.1.call-done.kv_ref = bf16[2048,384]{1,0:T(8,128)(2,1)} async-done(((bf16[256,384]{1,0:T(8,128)(2,1)}), bf16[2048,384]{1,0:T(8,128)(2,1)}) %all-gather.4.cloned.1.call-update) | async-done | bytes 1572880 | tf_op jit(solution)/shard_map/all_gather | solution.py:95
  64.1 0.0 all-gather.8.cloned.1.call-start
  64.2 23.6 %all_to_all.20 = bf16[8,24,2048]{2,1,0:T(8,128)(2,1)} all-to-all(bf16[8,24,2048]{2,1,0:T(8,128)(2,1)} %bitcast.94), channel_id=1, replica_groups=mesh['ep'=8,'tp'=4] {'ep'}, dimensions={0} | all-to-all | bytes 1572864 | tf_op jit(solution)/shard_map/all_to_all | solution.py:184
  87.8 0.0 reduce-scatter.4.cloned.1.call-start
  87.9 4.7 %all-gather.6.cloned.1.call-done = bf16[768,2048]{1,0:T(8,128)(2,1)} async-done(((bf16[192,2048]{1,0:T(8,128)(2,1)}), bf16[768,2048]{1,0:T(8,128)(2,1)}) %all-gather.6.cloned.1.call-update) | async-done | bytes 3145744 | tf_op jit(solution)/shard_map/all_gather | solution.py:188
  92.6 7.9 %fusion.6 = f32[768,896]{1,0:T(8,128)} fusion(bf16[768,2048]{1,0:T(8,128)(2,1)} %all-gather.6.cloned.1.call-done, bf16[1,2048,896]{2,1,0:T(8,128)(2,1)} %param.24), kind=kOutput, calls=%fused_computation.6 | convolution fusion | flops 2818572288 | bytes 9568256 | tf_op jit(solution)/shard_map/dot_general | solution.py:192
  100.5 12.9 %fusion.12 = bf16[768,2048]{1,0:T(8,128)(2,1)} fusion(bf16[1,896,2048]{2,1,0:T(8,128)(2,1)} %param.25, f32[768,896]{1,0:T(8,128)} %fusion.6, bf16[768,2048]{1,0:T(8,128)(2,1)} %all-gather.6.cloned.1.call-done, bf16[1,2048,896]{2,1,0:T(8,128)(2,1)} %param.23), kind=kOutput, calls=%fused_computation.12 | convolution fusion | flops 5642846208 | bytes 16384000 | tf_op jit(solution)/shard_map/dot_general | solution.py:194
  113.4 0.2 reduce-scatter.8.cloned.1.call-start
  113.6 9.1 %all-gather.8.cloned.1.call-done = bf16[768,2048]{1,0:T(8,128)(2,1)} async-done(((bf16[192,2048]{1,0:T(8,128)(2,1)}), bf16[768,2048]{1,0:T(8,128)(2,1)}) %all-gather.8.cloned.1.call-update) | async-done | bytes 3145744 | tf_op jit(solution)/shard_map/all_gather | solution.py:188
  122.7 7.9 %fusion.4 = f32[768,896]{1,0:T(8,128)} fusion(bf16[768,2048]{1,0:T(8,128)(2,1)} %all-gather.8.cloned.1.call-done, bf16[1,2048,896]{2,1,0:T(8,128)(2,1)} %param.24), kind=kOutput, calls=%fused_computation.4 | convolution fusion | flops 2818572288 | bytes 9568256 | tf_op jit(solution)/shard_map/dot_general | solution.py:192
  130.6 13.2 %fusion.15 = bf16[768,2048]{1,0:T(8,128)(2,1)} fusion(bf16[1,896,2048]{2,1,0:T(8,128)(2,1)} %param.25, f32[768,896]{1,0:T(8,128)} %fusion.4, bf16[768,2048]{1,0:T(8,128)(2,1)} %all-gather.8.cloned.1.call-done, bf16[1,2048,896]{2,1,0:T(8,128)(2,1)} %param.23), kind=kOutput, calls=%fused_computation.13 | convolution fusion | flops 5642846208 | bytes 16384000 | tf_op jit(solution)/shard_map/dot_general | solution.py:194
  143.8 0.6 copy-done.7
  144.4 0.1 pad_maximum_fusion.1
  144.5 0.1 copy.59
  144.6 0.1 copy-done.4
  144.7 0.1 copy.58
  144.9 0.1 broadcast_in_dim.48
  145.0 0.1 maximum_maximum_fusion
  145.1 0.3 copy.60
  145.4 1.4 copy-done.1
  146.8 3.8 %stick.1 = bf16[256,512]{1,0:T(8,128)(2,1)S(1)} custom-call(bf16[2048,128]{1,0:T(8,128)(2,1)S(1)} %bitcast.91, bf16[2048,384]{1,0:T(8,128)(2,1)S(1)} %copy-done.1, bf16[256,256]{1,0:T(8,128)(2,1)S(1)} %fusion.30.tri_ref), custom_call_target="tpu_custom_call" | custom-call | flops 4194304000 | bytes 1572864 | tf_op jit(solution)/shard_map/stick/pallas_call | solution.py:122
  150.6 12.3 %reduce-scatter.4.cloned.1.call-done = bf16[192,2048]{1,0:T(8,128)(2,1)} async-done(((bf16[768,2048]{1,0:T(8,128)(2,1)}), bf16[192,2048]{1,0:T(8,128)(2,1)}) %reduce-scatter.4.cloned.1.call-update) | async-done | bytes 786448 | tf_op jit(solution)/shard_map/reduce_scatter | solution.py:200
  163.0 18.6 %all-to-all-start.2 = ((bf16[8,24,2048]{2,1,0:T(8,128)(2,1)}), bf16[8,24,2048]{2,1,0:T(8,128)(2,1)}, u32[]{:S(2)}, u32[]{:S(2)}) async-start(bf16[8,24,2048]{2,1,0:T(8,128)(2,1)} %bitcast.98), calls=%async_computation.4 | async-start | bytes 1572864 | tf_op jit(solution)/shard_map/all_to_all | solution.py:212
  181.5 21.7 %reduce-scatter.8.cloned.1.call-done = bf16[192,2048]{1,0:T(8,128)(2,1)} async-done(((bf16[768,2048]{1,0:T(8,128)(2,1)}), bf16[192,2048]{1,0:T(8,128)(2,1)}) %reduce-scatter.8.cloned.1.call-update) | async-done | bytes 786448 | tf_op jit(solution)/shard_map/reduce_scatter | solution.py:200
  203.3 5.5 %all-to-all-start.3 = ((bf16[8,24,2048]{2,1,0:T(8,128)(2,1)}), bf16[8,24,2048]{2,1,0:T(8,128)(2,1)}, u32[]{:S(2)}, u32[]{:S(2)}) async-start(bf16[8,24,2048]{2,1,0:T(8,128)(2,1)} %bitcast.97), calls=%async_computation.6 | async-start | bytes 1572864 | tf_op jit(solution)/shard_map/all_to_all | solution.py:212
  208.8 0.0 reduce-scatter.6.cloned.1.call-start
  208.9 1.7 convolution_convert_fusion
  210.6 0.1 fusion.31
  210.7 1.5 fusion.41
  212.2 1.5 convolution_add_fusion.4
  213.7 1.5 convolution_add_fusion.3
  215.1 13.9 %all-to-all-done.3 = bf16[8,24,2048]{2,1,0:T(8,128)(2,1)} async-done(((bf16[8,24,2048]{2,1,0:T(8,128)(2,1)}), bf16[8,24,2048]{2,1,0:T(8,128)(2,1)}, u32[]{:S(2)}, u32[]{:S(2)}) %all-to-all-start.3) | async-done | bytes 786464 | tf_op jit(solution)/shard_map/all_to_all | solution.py:212
  229.0 1.5 convolution_add_fusion.2
  230.5 1.5 convolution_add_fusion.1
  231.9 2.3 fusion.18
  234.2 3.5 %reduce-scatter.6.cloned.1.call-done = bf16[64,2048]{1,0:T(8,128)(2,1)} async-done(((bf16[256,2048]{1,0:T(8,128)(2,1)}), bf16[64,2048]{1,0:T(8,128)(2,1)}) %reduce-scatter.6.cloned.1.call-update) | async-done | bytes 262160 | tf_op jit(solution)/shard_map/reduce_scatter | solution.py:204
  (32 shorter events, 0.3 us)
Async XLA Ops:
  7.2 201.7 %copy-start = (bf16[512,2048]{1,0:T(8,128)(2,1)S(1)}, bf16[512,2048]{1,0:T(8,128)(2,1)}, u32[]{:S(2)}) copy-start(bf16[512,2048]{1,0:T(8,128)(2,1)} %param.18) | copy-start | bytes 6291460
  7.2 18.2 %copy-start.2 = (bf16[128,2048]{1,0:T(8,128)(2,1)S(1)}, bf16[128,2048]{1,0:T(8,128)(2,1)}, u32[]{:S(2)}) copy-start(bf16[128,2048]{1,0:T(8,128)(2,1)} %param.19) | copy-start | bytes 1572868
  7.2 18.2 %copy-start.5 = (f32[2048]{0:T(1024)S(1)}, f32[2048]{0:T(1024)}, u32[]{:S(2)}) copy-start(f32[2048]{0:T(1024)} %param.20) | copy-start | bytes 24580
  7.2 56.9 %all-gather.4.cloned.1.call-start = ((), (), s32[]{:S(2)}) async-start(), calls=%async_computation.7 | async-start | bytes 1769472 | tf_op jit(solution)/shard_map/all_gather | solution.py:95
  18.0 34.4 %all-to-all-start = ((bf16[8,24,2048]{2,1,0:T(8,128)(2,1)}), bf16[8,24,2048]{2,1,0:T(8,128)(2,1)S(1)}, u32[]{:S(2)}, u32[]{:S(2)}) async-start(bf16[8,24,2048]{2,1,0:T(8,128)(2,1)} %bitcast.95), calls=%async_computation | async-start | bytes 1572864 | tf_op jit(solution)/shard_map/all_to_all | solution.py:184
  25.3 67.2 %all-gather.6.cloned.1.call-start = ((), (), s32[]{:S(2)}) async-start(), calls=%async_computation.8 | async-start | bytes 3932160 | tf_op jit(solution)/shard_map/all_gather | solution.py:188
  52.5 11.6 %copy-start.3 = (bf16[8,24,2048]{2,1,0:T(8,128)(2,1)}, bf16[8,24,2048]{2,1,0:T(8,128)(2,1)S(1)}, u32[]{:S(2)}) copy-start(bf16[8,24,2048]{2,1,0:T(8,128)(2,1)S(1)} %all-to-all-done) | copy-start | bytes 2359300
  64.1 58.5 %all-gather.8.cloned.1.call-start = ((), (), s32[]{:S(2)}) async-start(), calls=%async_computation.10 | async-start | bytes 3932160 | tf_op jit(solution)/shard_map/all_gather | solution.py:188
  87.8 75.1 %reduce-scatter.4.cloned.1.call-start = ((), (), s32[]{:S(2)}) async-start(), calls=%async_computation.9 | async-start | bytes 3932160 | tf_op jit(solution)/shard_map/reduce_scatter | solution.py:200
  113.4 89.9 %reduce-scatter.8.cloned.1.call-start = ((), (), s32[]{:S(2)}) async-start(), calls=%async_computation.12 | async-start | bytes 3932160 | tf_op jit(solution)/shard_map/reduce_scatter | solution.py:200
  143.8 0.7 copy-start.7
  143.8 1.0 copy-start.4
  145.4 1.4 copy-start.1
  163.0 40.3 %all-to-all-start.2 = ((bf16[8,24,2048]{2,1,0:T(8,128)(2,1)}), bf16[8,24,2048]{2,1,0:T(8,128)(2,1)}, u32[]{:S(2)}, u32[]{:S(2)}) async-start(bf16[8,24,2048]{2,1,0:T(8,128)(2,1)} %bitcast.98), calls=%async_computation.4 | async-start | bytes 1572864 | tf_op jit(solution)/shard_map/all_to_all | solution.py:212
  181.5 29.1 %copy-start.6 = (f32[128,2]{0,1:T(2,128)S(1)}, f32[128,2]{0,1:T(2,128)}, u32[]{:S(2)}) copy-start(f32[128,2]{0,1:T(2,128)} %param.22) | copy-start | bytes 3076
  203.3 25.7 %all-to-all-start.3 = ((bf16[8,24,2048]{2,1,0:T(8,128)(2,1)}), bf16[8,24,2048]{2,1,0:T(8,128)(2,1)}, u32[]{:S(2)}, u32[]{:S(2)}) async-start(bf16[8,24,2048]{2,1,0:T(8,128)(2,1)} %bitcast.97), calls=%async_computation.6 | async-start | bytes 1572864 | tf_op jit(solution)/shard_map/all_to_all | solution.py:212
  208.8 28.9 %reduce-scatter.6.cloned.1.call-start = ((), (), s32[]{:S(2)}) async-start(), calls=%async_computation.11 | async-start | bytes 1310720 | tf_op jit(solution)/shard_map/reduce_scatter | solution.py:204
Sparse Core Ops, SparseCore 0:
  11.1 52.9 all-gather.3
  65.7 26.8 all-gather.5
  94.1 28.4 all-gather.7
  125.1 37.8 reduce-scatter.3
  165.4 37.8 reduce-scatter.7
  212.4 25.2 reduce-scatter.5
where the time goes:
time: 245 us
  waiting for transfers between devices  103 us (42%)
  matrix products  56.9 us (23%)
  starting transfers between devices  31.8 us (13%)
  blocking collectives  23.6 us (10%)
  between operations  14.4 us (6%)
  local copies, waits for them, and re-layouts  6.41 us (3%)
  other arithmetic  4.95 us (2%)
  Pallas kernels  3.82 us (2%)
    reduce_scatter x2, waiting for transfers between devices, body(): lax.psum_scatter(partial_sum, 'tp', scatter_dimension=0, tiled=True)  34.1 us
    dot_general x2, matrix products, body(): jnp.dot(hidden_all, down_weight[0], preferred_element_type=jnp.float32)  26.1 us
    all_to_all x1, waiting for transfers between devices, body(): lax.all_to_all(outgoing, 'ep', split_axis=0, concat_axis=0, tiled=True)  25.7 us
    all_to_all x2, starting transfers between devices, body(): lax.all_to_all(results[chunk].reshape(expert_count, piece, model_width),...  24.1 us
    all_to_all x1, blocking collectives, body(): lax.all_to_all(outgoing, 'ep', split_axis=0, concat_axis=0, tiled=True)  23.6 us
    dot_general x2, matrix products, body(): jnp.dot(row_piece, up_weight[0], preferred_element_type=jnp.float32)  15.8 us
    all_to_all x2, waiting for transfers between devices, body(): lax.all_to_all(results[chunk].reshape(expert_count, piece, model_width),...  13.9 us
    all_gather x2, waiting for transfers between devices, body(): lax.all_gather(arrived[chunk].reshape(chunk_rows, model_width), 'tp', axi...  13.8 us
  transfers between devices with their start and end apart: 9, of which 8 were waited for; matrix products, arithmetic and copies ran while one was open for 26% of the time, Pallas kernels for 2%

commit v1 on v0

v1 whole, which is shorter than its diff:
```python
import functools
import math

import jax
import jax.numpy as jnp
from jax import lax
from jax.experimental import pallas as pl
from jax.experimental.pallas import tpu as pltpu
from jax.sharding import PartitionSpec as P

HD = 64
EPSILON = 1e-06
LOG2E = 1.4426950408889634
MESH = pl.DeviceIdType.MESH
CORES = 2
AHEAD = 3


def xor(a, b, size):
    total, bit = 0, 1
    while bit < size:
        total = total + bit * ((a // bit + b // bit) % 2)
        bit *= 2
    return total


def step_kernel(
    q_ref, k_ref, v_ref, bias_ref, offset_ref, x_ref, gain_ref, slot_rows_ref, slot_cols_ref, mix_ref,
    wo_hbm, wg_hbm, wu_hbm, wd_hbm,
    out_a_ref, out_b_ref,
    qw, kbuf, vbuf, bbuf, acc, carry, heads_out, tri,
    outgoing, rows, hidden, part, got, sum_out, sum_in, back_out, back_in,
    part_a, got_a, sum_out_a, sum_in_a,
    wgu, wd, wo,
    w_sem, kv_zsend, kv_psend, kv_recv,
    d_send, d_recv, x_send, x_recv, c_send, c_recv, p_send, p_recv, s_send, s_recv, b_send, b_recv,
    a_send, a_recv,
    *, ep, chunks, group_size, kv_local,
):
    me = lax.axis_index("ep")
    t = lax.axis_index("tp")
    c = t % CORES
    x = t // CORES
    mate = {"tp": CORES * x + 1 - c}
    across = {"tp": CORES * (1 - x) + c}
    per = ep // chunks
    cap = outgoing.shape[1]
    width = outgoing.shape[2]
    block = k_ref.shape[0]
    heads = kv_local * group_size
    up = me // 2
    upper = ep // 2
    odd = me % 2
    pair = me + 1 - 2 * odd

    def remote(src, dst, send, recv, device):
        return pltpu.make_async_remote_copy(
            src_ref=src, dst_ref=dst, send_sem=send, recv_sem=recv, device_id=device, device_id_type=MESH
        )

    tiles = wgu.shape[0]
    half = wgu.shape[2] // 2

    def weight_copies():
        copies = []
        for tile in range(tiles):
            lanes = slice(tile * half, (tile + 1) * half)
            copies.append(pltpu.make_async_copy(wg_hbm.at[0, :, lanes], wgu.at[tile, :, 0:half], w_sem.at[2 * tile]))
            copies.append(
                pltpu.make_async_copy(wu_hbm.at[0, :, lanes], wgu.at[tile, :, half : 2 * half], w_sem.at[2 * tile + 1])
            )
        copies.append(pltpu.make_async_copy(wd_hbm.at[0], wd, w_sem.at[2 * tiles]))
        return copies

    wo_copy = pltpu.make_async_copy(wo_hbm, wo, w_sem.at[2 * tiles + 1])
    wo_copy.start()
    for copy in weight_copies():
        copy.start()

    barrier = pltpu.get_barrier_semaphore()

    def greet(step, unused):
        pl.semaphore_signal(barrier, inc=1, device_id={"ep": (me + step) % ep}, device_id_type=MESH)
        return unused

    lax.fori_loop(1, ep, greet, 0)
    pl.semaphore_signal(barrier, inc=1, device_id=mate, device_id_type=MESH)
    pl.semaphore_signal(barrier, inc=1, device_id=across, device_id_type=MESH)
    pl.semaphore_wait(barrier, ep + 1)

    def own_kv(target, sems):
        return [
            remote(k_ref, kbuf.at[me], sems.at[0], kv_recv.at[me, 0], {"ep": target}),
            remote(v_ref, vbuf.at[me], sems.at[1], kv_recv.at[me, 1], {"ep": target}),
            remote(bias_ref, bbuf.at[me], sems.at[2], kv_recv.at[me, 2], {"ep": target}),
        ]

    def passed_kv(source, target):
        return [
            remote(ref.at[source], ref.at[source], kv_psend.at[source, i], kv_recv.at[source, i], {"ep": target})
            for i, ref in enumerate((kbuf, vbuf, bbuf))
        ]

    @pl.when(odd == 0)
    def _():
        for copy in own_kv(pair, kv_psend.at[me]):
            copy.start()

    def send_up(step, unused):
        for copy in own_kv(me + 2 * step, kv_zsend.at[step]):
            copy.start()
        return unused

    lax.fori_loop(1, upper - up, send_up, 0)

    values = x_ref[...].astype(jnp.float32)
    scale = lax.rsqrt(jnp.mean(values * values, axis=-1, keepdims=True) + EPSILON)
    normed = (values * scale * gain_ref[...]).astype(jnp.bfloat16)
    tok = normed.shape[0]
    ids = lax.broadcasted_iota(jnp.int32, (ep * cap, tok), 0)
    hit = (ids == slot_rows_ref[0:1, :]) | (ids == slot_rows_ref[1:2, :])
    hit = jnp.where(hit, 1.0, 0.0).astype(jnp.bfloat16)
    strip = 512
    for lane in range(0, width, strip):
        picked = jnp.dot(hit, normed[:, lane : lane + strip], preferred_element_type=jnp.float32)
        outgoing[:, :, lane : lane + strip] = picked.astype(jnp.bfloat16).reshape(ep, cap, strip)
    rows[0, c, 0, x] = outgoing[0]

    def slot_of(d):
        return rows.at[d // per, c, d % per, x]

    def dispatch(d):
        return remote(outgoing.at[d], slot_of(d), d_send.at[d], d_recv.at[d], {"ep": xor(me, d, ep)})

    def issue(d, unused):
        dispatch(d).start()
        return unused

    lax.fori_loop(1, 1 + AHEAD, issue, 0)

    lane_ids = lax.broadcasted_iota(jnp.int32, (kv_local * HD, kv_local * HD), 1)
    row_ids = lax.broadcasted_iota(jnp.int32, (kv_local * HD, kv_local * HD), 0)
    wide = kv_local * HD
    for head in range(heads):
        kv = head // group_size
        first = head * HD // wide * wide
        shift = head * HD - first - kv * HD
        move = jnp.where((row_ids == lane_ids + shift) & (lane_ids // HD == kv), 1.0, 0.0).astype(jnp.bfloat16)
        qw[head] = jnp.dot(
            q_ref[:, first : first + wide], move, preferred_element_type=jnp.float32
        ).astype(jnp.bfloat16)
    key_ids = lax.broadcasted_iota(jnp.int32, (block, block), 0)
    place = lax.broadcasted_iota(jnp.int32, (block, block), 1)
    tri[...] = jnp.where(key_ids > place, 1.0, 0.0).astype(jnp.bfloat16)
    acc[...] = jnp.zeros_like(acc)
    carry[...] = jnp.zeros_like(carry)

    def tile(keys, vals, biases, keep):
        for head in range(heads):
            kv = head // group_size
            raw = lax.dot_general(
                qw[head], keys[...], (((1,), (1,)), ((), ())), preferred_element_type=jnp.float32
            )
            row = (biases[kv : kv + 1, :].astype(jnp.float32) + offset_ref[head]) * LOG2E
            scores = raw * (LOG2E / math.sqrt(HD)) + row
            soft = jnp.log2(1.0 + jnp.exp2(-jnp.abs(scores)))
            leave = jnp.maximum(scores, 0.0) + soft
            log_take = jnp.minimum(scores, 0.0) - soft
            if keep is not None:
                leave = jnp.where(keep, leave, 0.0)
            high = leave.astype(jnp.bfloat16)
            low = (leave - high.astype(jnp.float32)).astype(jnp.bfloat16)
            after = jnp.dot(high, tri[...], preferred_element_type=jnp.float32) + jnp.dot(
                low, tri[...], preferred_element_type=jnp.float32
            )
            before = carry[head]
            weights = jnp.exp2(log_take - after - before)
            if keep is not None:
                weights = jnp.where(keep, weights, 0.0)
            acc[head] += jnp.dot(weights.astype(jnp.bfloat16), vals[...], preferred_element_type=jnp.float32)
            carry[head] = before + after[:, :1] + leave[:, :1]

    def wait_kv(source):
        for i, ref in enumerate((kbuf, vbuf, bbuf)):
            remote(ref.at[source], ref.at[source], kv_psend.at[source, i], kv_recv.at[source, i], mate).wait_recv()

    def project():
        lanes = slice(0, 0)
        pieces = []
        for head in range(heads):
            kv = head // group_size
            lanes = slice(kv * HD, (kv + 1) * HD)
            pieces.append(acc[head, :, lanes].astype(jnp.bfloat16))
        for head in range(heads):
            heads_out[:, head * HD : (head + 1) * HD] = pieces[head]
        own = part_a.shape[2]
        for lane in range(0, width, strip):
            value = jnp.dot(heads_out[...], wo[:, lane : lane + strip], preferred_element_type=jnp.float32)
            value = value.astype(jnp.bfloat16).reshape(2, CORES, own, strip)
            for xs in range(2):
                for cs in range(CORES):
                    part_a[cs, xs, :, lane : lane + strip] = value[xs, cs]

    def send_a():
        return remote(part_a.at[1 - c], got_a, a_send.at[0], a_recv.at[0], mate)

    def cross_a():
        return remote(sum_out_a, sum_in_a, a_send.at[1], a_recv.at[1], across)

    def experts(k):
        flat_rows = part.shape[1] * part.shape[2] * part.shape[3] * cap

        def gate_up(j, unused):
            both = jnp.dot(
                rows[k].reshape(flat_rows, width), wgu[j], preferred_element_type=jnp.float32
            )
            gate = both[:, :half]
            hidden[:, pl.ds(pl.multiple_of(j * half, half), half)] = (
                gate / (1.0 + jnp.exp(-gate)) * both[:, half:]
            ).astype(jnp.bfloat16)
            return unused

        lax.fori_loop(0, tiles, gate_up, 0)

        def down(j, unused):
            lanes = pl.ds(pl.multiple_of(j * strip, strip), strip)
            value = jnp.dot(hidden[...], wd[:, lanes], preferred_element_type=jnp.float32)
            part[k, :, :, :, :, lanes] = value.astype(jnp.bfloat16).reshape(part.shape[1:5] + (strip,))
            return unused

        lax.fori_loop(0, width // strip, down, 0)

    def send_p(k):
        return remote(part.at[k, 1 - c], got.at[k], p_send.at[k], p_recv.at[k], mate)

    def cross_p(k):
        return remote(sum_out.at[k], sum_in.at[k], s_send.at[k], s_recv.at[k], across)

    def send_back(k, i):
        d = k * per + i
        return remote(back_out.at[d], back_in.at[d], b_send.at[d], b_recv.at[d], {"ep": xor(me, d, ep)})

    def forward_x(d):
        return remote(slot_of(d), slot_of(d), x_send.at[d], x_recv.at[d], across)

    def forward_c(d):
        return remote(slot_of(d), slot_of(d), c_send.at[d, 0], c_recv.at[d, 0], mate)

    def forward_xc(d):
        ref = rows.at[d // per, c, d % per, 1 - x]
        return remote(ref, ref, c_send.at[d, 1], c_recv.at[d, 1], mate)

    first_chunk = per + 1

    def step(i, unused):
        @pl.when(i < ep)
        def _():
            @pl.when(i > 0)
            def _():
                dispatch(i).wait_recv()

            forward_x(i).start()
            forward_c(i).start()

        @pl.when((i > 0) & (i <= ep))
        def _():
            forward_x(i - 1).wait_recv()
            forward_xc(i - 1).start()

        @pl.when(i + AHEAD + 1 < ep)
        def _():
            dispatch(i + AHEAD + 1).start()

        lag = i - first_chunk - 2
        @pl.when((lag >= 0) & (lag % per == 0) & (lag // per < chunks))
        def _():
            k = lag // per
            cross_p(k).wait_recv()

            def finish(n, unused):
                total = (
                    part[k, c, n, x].astype(jnp.float32)
                    + got[k, n, x].astype(jnp.float32)
                    + sum_in[k, n].astype(jnp.float32)
                )
                back_out[k * per + n] = total.astype(jnp.bfloat16)

                @pl.when(k * per + n > 0)
                def _():
                    send_back(k, n).start()

                return unused

            lax.fori_loop(0, per, finish, 0)

        lag1 = i - first_chunk - 1
        @pl.when((lag1 >= 0) & (lag1 % per == 0) & (lag1 // per < chunks))
        def _():
            k = lag1 // per
            send_p(k).wait_recv()

            def add(n, unused):
                total = part[k, c, n, 1 - x].astype(jnp.float32) + got[k, n, 1 - x].astype(jnp.float32)
                sum_out[k, n] = total.astype(jnp.bfloat16)
                return unused

            lax.fori_loop(0, per, add, 0)
            cross_p(k).start()

        @pl.when(i == 0)
        def _():
            tile(k_ref, v_ref, bias_ref, place < key_ids)

        @pl.when((i > 0) & (i <= me))
        def _():
            source = me - i

            @pl.when(i % 2 == 1)
            def _():
                wait_kv(source)

            tile(kbuf.at[source], vbuf.at[source], bbuf.at[source], None)

        @pl.when((i % 2 == 0) & (i + 2 <= me))
        def _():
            wait_kv(me - i - 2)
            for copy in passed_kv(me - i - 2, pair):
                copy.start()

        @pl.when(i == me)
        def _():
            wo_copy.wait()
            project()
            send_a().start()

        @pl.when(i == me + 1)
        def _():
            send_a().wait_recv()
            sum_out_a[...] = (
                part_a[c, 1 - x].astype(jnp.float32) + got_a[1 - x].astype(jnp.float32)
            ).astype(jnp.bfloat16)
            cross_a().start()

        @pl.when(i == me + 3)
        def _():
            cross_a().wait_recv()
            out_a_ref[...] = (
                part_a[c, x].astype(jnp.float32) + got_a[x].astype(jnp.float32) + sum_in_a[...].astype(jnp.float32)
            ).astype(jnp.bfloat16)

        lag0 = i - first_chunk
        @pl.when((lag0 >= 0) & (lag0 % per == 0) & (lag0 // per < chunks))
        def _():
            k = lag0 // per

            @pl.when(k == 0)
            def _():
                for copy in weight_copies():
                    copy.wait()

            def landed(n, unused):
                forward_c(k * per + n).wait_recv()
                forward_xc(k * per + n).wait_recv()
                return unused

            lax.fori_loop(0, per, landed, 0)
            experts(k)
            send_p(k).start()

        return unused

    lax.fori_loop(0, first_chunk + (chunks - 1) * per + 3, step, 0)

    back_in[0] = back_out[0]

    def returned(d, unused):
        remote(back_out.at[d], back_in.at[d], b_send.at[d], b_recv.at[d], mate).wait_recv()
        return unused

    lax.fori_loop(1, ep, returned, 0)
    spots = lax.broadcasted_iota(jnp.int32, (tok, ep * cap), 1)
    share = jnp.zeros((tok, ep * cap), jnp.float32)
    for choice in range(slot_cols_ref.shape[1]):
        share = share + jnp.where(spots == slot_cols_ref[:, choice : choice + 1], mix_ref[:, choice : choice + 1], 0.0)
    high = share.astype(jnp.bfloat16)
    rest = share - high.astype(jnp.float32)
    low = rest.astype(jnp.bfloat16)
    for lane in range(0, width, strip):
        piece = back_in[:, :, lane : lane + strip].reshape(ep * cap, strip)
        out_b_ref[:, lane : lane + strip] = (
            jnp.dot(high, piece, preferred_element_type=jnp.float32)
            + jnp.dot(low, piece, preferred_element_type=jnp.float32)
        ).astype(jnp.bfloat16)

    @pl.when(odd == 0)
    def _():
        for copy in own_kv(pair, kv_psend.at[me]):
            copy.wait_send()

    def left_up(step, unused):
        for copy in own_kv(me + 2 * step, kv_zsend.at[step]):
            copy.wait_send()
        return unused

    lax.fori_loop(1, upper - up, left_up, 0)

    def left_pair(step, unused):
        for copy in passed_kv(me - 2 * step, pair):
            copy.wait_send()
        return unused

    lax.fori_loop(1, up + 1, left_pair, 0)

    def left_rows(d, unused):
        @pl.when(d > 0)
        def _():
            dispatch(d).wait_send()
            send_back(d // per, d % per).wait_send()

        forward_x(d).wait_send()
        forward_c(d).wait_send()
        forward_xc(d).wait_send()
        return unused

    lax.fori_loop(0, ep, left_rows, 0)

    def left_sums(k, unused):
        send_p(k).wait_send()
        cross_p(k).wait_send()
        return unused

    lax.fori_loop(0, chunks, left_sums, 0)
    send_a().wait_send()
    cross_a().wait_send()


def body(
    query_rows,
    key_rows,
    value_rows,
    key_bias,
    head_offset,
    out_weight,
    expert_input,
    expert_gain,
    routes,
    route_weight,
    gate_weight,
    up_weight,
    down_weight,
):
    ep, tp = lax.axis_size("ep"), lax.axis_size("tp")
    me = lax.axis_index("ep")
    block = key_rows.shape[0]
    kv_local = key_rows.shape[1] // HD
    heads = query_rows.shape[1] // HD
    tok, width = expert_input.shape
    top = routes.shape[1]
    hidden_width = gate_weight.shape[2]
    cap = max(2, 3 * tok * top // (2 * ep))
    cap = -(-cap // 16) * 16
    chunks = 4
    per = ep // chunks
    across = tp // CORES
    flat = routes.reshape(-1)
    order = jnp.arange(flat.shape[0])
    rank = jnp.sum((flat[:, None] == flat[None, :]) & (order[None, :] < order[:, None]), axis=1, dtype=jnp.int32)
    slots = ((flat ^ me) * cap + rank).reshape(tok, top)
    bias = jnp.pad(key_bias.T, ((0, 16 - kv_local), (0, 0)))
    half = 128
    tiles = hidden_width // half
    vmem = pl.BlockSpec(memory_space=pltpu.VMEM)
    hbm = pl.BlockSpec(memory_space=pl.ANY)
    bf16, f32, dma = jnp.bfloat16, jnp.float32, pltpu.SemaphoreType.DMA
    own_a = block // tp
    wide = kv_local * HD
    return pl.pallas_call(
        functools.partial(step_kernel, ep=ep, chunks=chunks, group_size=heads // kv_local, kv_local=kv_local),
        out_shape=(
            jax.ShapeDtypeStruct((own_a, width), bf16),
            jax.ShapeDtypeStruct((tok, width), bf16),
        ),
        in_specs=[vmem] * 4 + [pl.BlockSpec(memory_space=pltpu.SMEM)] + [vmem] * 5 + [hbm] * 4,
        out_specs=(vmem, vmem),
        scratch_shapes=[
            pltpu.VMEM((heads, block, wide), bf16),
            pltpu.VMEM((ep, block, wide), bf16),
            pltpu.VMEM((ep, block, wide), bf16),
            pltpu.VMEM((ep, 16, block), bf16),
            pltpu.VMEM((heads, block, wide), f32),
            pltpu.VMEM((heads, block, 1), f32),
            pltpu.VMEM((block, heads * HD), bf16),
            pltpu.VMEM((block, block), bf16),
            pltpu.VMEM((ep, cap, width), bf16),
            pltpu.VMEM((chunks, CORES, per, across, cap, width), bf16),
            pltpu.VMEM((CORES * per * across * cap, hidden_width), bf16),
            pltpu.VMEM((chunks, CORES, per, across, cap, width), bf16),
            pltpu.VMEM((chunks, per, across, cap, width), bf16),
            pltpu.VMEM((chunks, per, cap, width), bf16),
            pltpu.VMEM((chunks, per, cap, width), bf16),
            pltpu.VMEM((ep, cap, width), bf16),
            pltpu.VMEM((ep, cap, width), bf16),
            pltpu.VMEM((CORES, across, own_a, width), bf16),
            pltpu.VMEM((across, own_a, width), bf16),
            pltpu.VMEM((own_a, width), bf16),
            pltpu.VMEM((own_a, width), bf16),
            pltpu.VMEM((tiles, width, 2 * half), bf16),
            pltpu.VMEM((hidden_width, width), bf16),
            pltpu.VMEM((heads * HD, width), bf16),
            dma((2 * tiles + 2,)),
            dma((ep // 2, 3)),
            dma((ep, 3)),
            dma((ep, 3)),
            dma((ep,)), dma((ep,)), dma((ep,)), dma((ep,)), dma((ep, 2)), dma((ep, 2)),
            dma((chunks,)), dma((chunks,)), dma((chunks,)), dma((chunks,)), dma((ep,)), dma((ep,)),
            dma((2,)), dma((2,)),
        ],
        compiler_params=pltpu.CompilerParams(
            collective_id=0, has_side_effects=True, vmem_limit_bytes=60 * 1024 * 1024
        ),
        name="step",
    )(
        query_rows, key_rows, value_rows, bias, head_offset, expert_input, expert_gain[None, :],
        slots.T, slots, route_weight, out_weight, gate_weight, up_weight, down_weight,
    )


def solution(mesh):
    return jax.shard_map(
        body,
        mesh=mesh,
        in_specs=(
            P("ep", "tp"),
            P("ep", "tp"),
            P("ep", "tp"),
            P("ep", "tp"),
            P("tp"),
            P("tp", None),
            P(("ep", "tp"), None),
            P(),
            P(("ep", "tp"), None),
            P(("ep", "tp"), None),
            P("ep", None, "tp"),
            P("ep", None, "tp"),
            P("ep", "tp", None),
        ),
        out_specs=(P(("ep", "tp"), None), P(("ep", "tp"), None)),
        check_vma=False,
    )
```

time: 245 us -> 150 us (0.61)
  the two profiles are of different devices: /device:TPU:0 before, /device:TPU:15 now
where the time goes in v1:
time: 150 us
  Pallas kernels  141 us (94%)
  local copies, waits for them, and re-layouts  7.96 us (5%)
    pallas_call x1, Pallas kernels, body(): pl.pallas_call(functools.partial(step_kernel, ep=ep, chunks=chunks, group...  141 us
    unnamed x6, local copies, waits for them, and re-layouts  5.75 us

profile of v1, /device:TPU:15, one launch (start us, length us, event | category | flops | bytes accessed | tf_op | source)
XLA Modules:
  0.0 149.7 jit_solution(16606535274117884990)
XLA Ops:
  0.6 1.3 pad.4.bias_ref
  1.9 0.8 copy.22
  2.7 0.1 eq.15
  2.8 0.2 convert_reduce_fusion
  3.0 0.1 reduce_sum.12
  3.2 0.0 copy-start
  3.2 0.6 copy.24.slot_rows_ref
  3.9 1.4 copy.25.mix_ref
  5.3 0.0 copy-done
  5.3 140.8 %step.1 = (bf16[64,2048]{1,0:T(8,128)(2,1)}, bf16[128,2048]{1,0:T(8,128)(2,1)}) custom-call(bf16[256,512]{1,0:T(8,128)(2,1)} %q_ref.1, bf16[256,128]{1,0:T(8,128)(2,1)} %k_ref.1, bf16[256,128]{1,0:T(8,128)(2,1)} %v_ref.1, bf16[16,256]{1,0:T(8,128)(2,1)} %pad.4.bias_ref, f32[8]{0:T(128)} %offset_ref.1, bf16[128,2048]{1,0:T(8,128)(2,1)} %x_ref.1, ...), custom_call_target="tpu_custom_call" | custom-call | tf_op jit(solution)/shard_map/step/pallas_call | solution.py:477
  146.1 1.7 %copy.28 = bf16[64,2048]{1,0:T(8,128)(2,1)} copy(bf16[64,2048]{1,0:T(8,128)(2,1)} %get-tuple-element.4) | data formatting | bytes 524288
  147.8 1.9 %copy.29 = bf16[128,2048]{1,0:T(8,128)(2,1)} copy(bf16[128,2048]{1,0:T(8,128)(2,1)} %get-tuple-element.5) | data formatting | bytes 1048576
  (1 shorter events, 0.0 us)
Async XLA Ops:
  3.2 2.1 %copy-start = (s32[128,2]{1,0:T(8,128)}, s32[128,2]{1,0:T(8,128)S(1)}, u32[]{:S(2)}) copy-start(s32[128,2]{1,0:T(8,128)S(1)} %multiply_add_fusion.slot_cols_ref) | copy-start | bytes 3076

commit v2 on v1

--- a/solution.py
+++ b/solution.py
@@ -13,7 +13,6 @@
 LOG2E = 1.4426950408889634
 MESH = pl.DeviceIdType.MESH
 CORES = 2
-AHEAD = 3
 
 
 def xor(a, b, size):
@@ -25,11 +24,11 @@
 
 
 def step_kernel(
-    q_ref, k_ref, v_ref, bias_ref, offset_ref, x_ref, gain_ref, slot_rows_ref, slot_cols_ref, mix_ref,
+    q_ref, k_ref, v_ref, bias_ref, offset_ref, x_ref, gain_ref, routes_ref, mix_ref,
     wo_hbm, wg_hbm, wu_hbm, wd_hbm,
     out_a_ref, out_b_ref,
     qw, kbuf, vbuf, bbuf, acc, carry, heads_out, tri,
-    outgoing, rows, hidden, part, got, sum_out, sum_in, back_out, back_in,
+    hit, share_high, share_low, outgoing, rows, hidden, part, got, sum_out, sum_in, back_out, back_in,
     part_a, got_a, sum_out_a, sum_in_a,
     wgu, wd, wo,
     w_sem, kv_zsend, kv_psend, kv_recv,
@@ -44,6 +43,7 @@
     mate = {"tp": CORES * x + 1 - c}
     across = {"tp": CORES * (1 - x) + c}
     per = ep // chunks
+    unit = per // 2
     cap = outgoing.shape[1]
     width = outgoing.shape[2]
     block = k_ref.shape[0]
@@ -77,6 +77,7 @@
     for copy in weight_copies():
         copy.start()
 
+    direct = range(1, per + per // 2)
     barrier = pltpu.get_barrier_semaphore()
 
     def greet(step, unused):
@@ -86,57 +87,28 @@
     lax.fori_loop(1, ep, greet, 0)
     pl.semaphore_signal(barrier, inc=1, device_id=mate, device_id_type=MESH)
     pl.semaphore_signal(barrier, inc=1, device_id=across, device_id_type=MESH)
-    pl.semaphore_wait(barrier, ep + 1)
-
-    def own_kv(target, sems):
-        return [
-            remote(k_ref, kbuf.at[me], sems.at[0], kv_recv.at[me, 0], {"ep": target}),
-            remote(v_ref, vbuf.at[me], sems.at[1], kv_recv.at[me, 1], {"ep": target}),
-            remote(bias_ref, bbuf.at[me], sems.at[2], kv_recv.at[me, 2], {"ep": target}),
-        ]
-
-    def passed_kv(source, target):
-        return [
-            remote(ref.at[source], ref.at[source], kv_psend.at[source, i], kv_recv.at[source, i], {"ep": target})
-            for i, ref in enumerate((kbuf, vbuf, bbuf))
-        ]
-
-    @pl.when(odd == 0)
-    def _():
-        for copy in own_kv(pair, kv_psend.at[me]):
-            copy.start()
-
-    def send_up(step, unused):
-        for copy in own_kv(me + 2 * step, kv_zsend.at[step]):
-            copy.start()
-        return unused
-
-    lax.fori_loop(1, upper - up, send_up, 0)
+    for d in direct:
+        device = {"ep": xor(me, d, ep), "tp": CORES * (1 - x) + c}
+        pl.semaphore_signal(barrier, inc=1, device_id=device, device_id_type=MESH)
 
     values = x_ref[...].astype(jnp.float32)
     scale = lax.rsqrt(jnp.mean(values * values, axis=-1, keepdims=True) + EPSILON)
     normed = (values * scale * gain_ref[...]).astype(jnp.bfloat16)
     tok = normed.shape[0]
-    ids = lax.broadcasted_iota(jnp.int32, (ep * cap, tok), 0)
-    hit = (ids == slot_rows_ref[0:1, :]) | (ids == slot_rows_ref[1:2, :])
-    hit = jnp.where(hit, 1.0, 0.0).astype(jnp.bfloat16)
+    bf16 = jnp.bfloat16
+    expert_ids = xor(lax.broadcasted_iota(jnp.int32, (ep, tok), 0), me, ep)
+    named = jnp.where((routes_ref[0:1, :] == expert_ids) | (routes_ref[1:2, :] == expert_ids), 1.0, 0.0)
+    earlier = lax.broadcasted_iota(jnp.int32, (tok, tok), 0) < lax.broadcasted_iota(jnp.int32, (tok, tok), 1)
+    rank = jnp.dot(named.astype(bf16), jnp.where(earlier, 1.0, 0.0).astype(bf16), preferred_element_type=jnp.float32)
+    rank = jnp.where(named > 0.0, rank, -1.0)
+    spots = lax.broadcasted_iota(jnp.int32, (cap, tok), 0).astype(jnp.float32)
+    for d in range(ep):
+        hit[d] = jnp.where(rank[d : d + 1, :] == spots, 1.0, 0.0).astype(bf16)
     strip = 512
     for lane in range(0, width, strip):
-        picked = jnp.dot(hit, normed[:, lane : lane + strip], preferred_element_type=jnp.float32)
+        picked = jnp.dot(hit[...].reshape(ep * cap, tok), normed[:, lane : lane + strip], preferred_element_type=jnp.float32)
         outgoing[:, :, lane : lane + strip] = picked.astype(jnp.bfloat16).reshape(ep, cap, strip)
     rows[0, c, 0, x] = outgoing[0]
-
-    def slot_of(d):
-        return rows.at[d // per, c, d % per, x]
-
-    def dispatch(d):
-        return remote(outgoing.at[d], slot_of(d), d_send.at[d], d_recv.at[d], {"ep": xor(me, d, ep)})
-
-    def issue(d, unused):
-        dispatch(d).start()
-        return unused
-
-    lax.fori_loop(1, 1 + AHEAD, issue, 0)
 
     lane_ids = lax.broadcasted_iota(jnp.int32, (kv_local * HD, kv_local * HD), 1)
     row_ids = lax.broadcasted_iota(jnp.int32, (kv_local * HD, kv_local * HD), 0)
@@ -154,6 +126,60 @@
     tri[...] = jnp.where(key_ids > place, 1.0, 0.0).astype(jnp.bfloat16)
     acc[...] = jnp.zeros_like(acc)
     carry[...] = jnp.zeros_like(carry)
+
+    pl.semaphore_wait(barrier, ep + 1 + len(direct))
+
+    def own_kv(target, sems):
+        return [
+            remote(k_ref, kbuf.at[me], sems.at[0], kv_recv.at[me, 0], {"ep": target}),
+            remote(v_ref, vbuf.at[me], sems.at[1], kv_recv.at[me, 1], {"ep": target}),
+            remote(bias_ref, bbuf.at[me], sems.at[2], kv_recv.at[me, 2], {"ep": target}),
+        ]
+
+    def passed_kv(source, target, sems):
+        return [
+            remote(ref.at[source], ref.at[source], sems.at[source, i], kv_recv.at[source, i], {"ep": target})
+            for i, ref in enumerate((kbuf, vbuf, bbuf))
+        ]
+
+    @pl.when(odd == 0)
+    def _():
+        for copy in own_kv(pair, kv_psend.at[me]):
+            copy.start()
+
+    @pl.when(up < upper - 1)
+    def _():
+        for copy in own_kv(me + 2, kv_zsend.at[me]):
+            copy.start()
+
+    groups = [range(k * per, (k + 1) * per) for k in range(chunks)]
+
+    def slot_of(d):
+        return rows.at[d // per, c, d % per, x]
+
+    def dispatch(d):
+        return remote(outgoing.at[d], slot_of(d), d_send.at[d], d_recv.at[d], {"ep": xor(me, d, ep)})
+
+    def dispatch_across(d):
+        device = {"ep": xor(me, d, ep), "tp": CORES * (1 - x) + c}
+        return remote(outgoing.at[d], slot_of(d), x_send.at[d], x_recv.at[d], device)
+
+    def forward_x(d):
+        return remote(slot_of(d), slot_of(d), x_send.at[d], x_recv.at[d], across)
+
+    def forward_c(d):
+        return remote(slot_of(d), slot_of(d), c_send.at[d, 0], c_recv.at[d, 0], mate)
+
+    def forward_xc(d):
+        ref = rows.at[d // per, c, d % per, 1 - x]
+        return remote(ref, ref, c_send.at[d, 1], c_recv.at[d, 1], mate)
+
+    forward_x(0).start()
+    forward_c(0).start()
+    for d in list(groups[0][1:]) + [d for pair_of in zip(groups[2], groups[1]) for d in pair_of]:
+        dispatch(d).start()
+        if d in direct:
+            dispatch_across(d).start()
 
     def tile(keys, vals, biases, keep):
         for head in range(heads):
@@ -226,86 +252,69 @@
             lanes = pl.ds(pl.multiple_of(j * strip, strip), strip)
             value = jnp.dot(hidden[...], wd[:, lanes], preferred_element_type=jnp.float32)
             part[k, :, :, :, :, lanes] = value.astype(jnp.bfloat16).reshape(part.shape[1:5] + (strip,))
+            send_p(k, j).start()
             return unused
 
         lax.fori_loop(0, width // strip, down, 0)
 
-    def send_p(k):
-        return remote(part.at[k, 1 - c], got.at[k], p_send.at[k], p_recv.at[k], mate)
-
-    def cross_p(k):
-        return remote(sum_out.at[k], sum_in.at[k], s_send.at[k], s_recv.at[k], across)
-
-    def send_back(k, i):
-        d = k * per + i
+    def send_p(k, j):
+        lanes = pl.ds(pl.multiple_of(j * strip, strip), strip)
+        return remote(
+            part.at[k, 1 - c, :, :, :, lanes], got.at[k, :, :, :, lanes], p_send.at[k, j], p_recv.at[k, j], mate
+        )
+
+    def cross_p(k, n):
+        return remote(sum_out.at[k, n], sum_in.at[k, n], s_send.at[k, n], s_recv.at[k, n], across)
+
+    def send_back(d):
         return remote(back_out.at[d], back_in.at[d], b_send.at[d], b_recv.at[d], {"ep": xor(me, d, ep)})
 
-    def forward_x(d):
-        return remote(slot_of(d), slot_of(d), x_send.at[d], x_recv.at[d], across)
-
-    def forward_c(d):
-        return remote(slot_of(d), slot_of(d), c_send.at[d, 0], c_recv.at[d, 0], mate)
-
-    def forward_xc(d):
-        ref = rows.at[d // per, c, d % per, 1 - x]
-        return remote(ref, ref, c_send.at[d, 1], c_recv.at[d, 1], mate)
-
-    first_chunk = per + 1
+    def own_rows(ds):
+        for d in ds:
+            dispatch(d).wait_recv()
+            if d not in direct:
+                forward_x(d).start()
+            forward_c(d).start()
+
+    def cross_rows(ds):
+        for d in ds:
+            forward_x(d).wait_recv()
+            forward_xc(d).start()
+
+    def first_sum(k):
+        for j in range(width // strip):
+            send_p(k, j).wait_recv()
+
+        def add(n, unused):
+            total = part[k, c, n, 1 - x].astype(jnp.float32) + got[k, n, 1 - x].astype(jnp.float32)
+            sum_out[k, n] = total.astype(jnp.bfloat16)
+            cross_p(k, n).start()
+            return unused
+
+        lax.fori_loop(0, per, add, 0)
+
+    def last_sum(k):
+        for n, d in enumerate(groups[k]):
+            cross_p(k, n).wait_recv()
+            total = (
+                part[k, c, n, x].astype(jnp.float32)
+                + got[k, n, x].astype(jnp.float32)
+                + sum_in[k, n].astype(jnp.float32)
+            )
+            back_out[d] = total.astype(jnp.bfloat16)
+            if d > 0:
+                send_back(d).start()
+
+    expert_steps = (unit, 3 * unit, 4 * unit, 6 * unit)
 
     def step(i, unused):
-        @pl.when(i < ep)
-        def _():
-            @pl.when(i > 0)
-            def _():
-                dispatch(i).wait_recv()
-
-            forward_x(i).start()
-            forward_c(i).start()
-
-        @pl.when((i > 0) & (i <= ep))
-        def _():
-            forward_x(i - 1).wait_recv()
-            forward_xc(i - 1).start()
-
-        @pl.when(i + AHEAD + 1 < ep)
-        def _():
-            dispatch(i + AHEAD + 1).start()
-
-        lag = i - first_chunk - 2
-        @pl.when((lag >= 0) & (lag % per == 0) & (lag // per < chunks))
-        def _():
-            k = lag // per
-            cross_p(k).wait_recv()
-
-            def finish(n, unused):
-                total = (
-                    part[k, c, n, x].astype(jnp.float32)
-                    + got[k, n, x].astype(jnp.float32)
-                    + sum_in[k, n].astype(jnp.float32)
-                )
-                back_out[k * per + n] = total.astype(jnp.bfloat16)
-
-                @pl.when(k * per + n > 0)
-                def _():
-                    send_back(k, n).start()
-
-                return unused
-
-            lax.fori_loop(0, per, finish, 0)
-
-        lag1 = i - first_chunk - 1
-        @pl.when((lag1 >= 0) & (lag1 % per == 0) & (lag1 // per < chunks))
-        def _():
-            k = lag1 // per
-            send_p(k).wait_recv()
-
-            def add(n, unused):
-                total = part[k, c, n, 1 - x].astype(jnp.float32) + got[k, n, 1 - x].astype(jnp.float32)
-                sum_out[k, n] = total.astype(jnp.bfloat16)
-                return unused
-
-            lax.fori_loop(0, per, add, 0)
-            cross_p(k).start()
+        @pl.when(i == 2 * unit)
+        def _():
+            own_rows(groups[2])
+
+        @pl.when(i == 4 * unit)
+        def _():
+            own_rows(groups[3])
 
         @pl.when(i == 0)
         def _():
@@ -323,9 +332,15 @@
 
         @pl.when((i % 2 == 0) & (i + 2 <= me))
         def _():
-            wait_kv(me - i - 2)
-            for copy in passed_kv(me - i - 2, pair):
+            source = me - i - 2
+            wait_kv(source)
+            for copy in passed_kv(source, pair, kv_psend):
                 copy.start()
+
+            @pl.when(up < upper - 1)
+            def _():
+                for copy in passed_kv(source, me + 2, kv_zsend):
+                    copy.start()
 
         @pl.when(i == me)
         def _():
@@ -341,35 +356,87 @@
             ).astype(jnp.bfloat16)
             cross_a().start()
 
-        @pl.when(i == me + 3)
-        def _():
-            cross_a().wait_recv()
-            out_a_ref[...] = (
-                part_a[c, x].astype(jnp.float32) + got_a[x].astype(jnp.float32) + sum_in_a[...].astype(jnp.float32)
-            ).astype(jnp.bfloat16)
-
-        lag0 = i - first_chunk
-        @pl.when((lag0 >= 0) & (lag0 % per == 0) & (lag0 // per < chunks))
-        def _():
-            k = lag0 // per
-
-            @pl.when(k == 0)
-            def _():
-                for copy in weight_copies():
-                    copy.wait()
+        @pl.when(i == expert_steps[0])
+        def _():
+            for copy in weight_copies():
+                copy.wait()
+
+        @pl.when(i == 0)
+        def _():
+            own_rows(groups[0][1:])
+
+        @pl.when(i == unit)
+        def _():
+            for d in groups[3]:
+                dispatch(d).start()
+            cross_rows(groups[0])
+
+        @pl.when(i == 3 * unit)
+        def _():
+            cross_rows(groups[2])
+
+        @pl.when(i == 4 * unit)
+        def _():
+            cross_rows(groups[1][per // 2 :])
+
+        @pl.when(i == 6 * unit)
+        def _():
+            cross_rows(groups[3])
+
+        @pl.when((i == expert_steps[0]) | (i == expert_steps[1]) | (i == expert_steps[2]) | (i == expert_steps[3]))
+        def _():
+            k = 0
+            for later, more in zip(expert_steps[1:], (2, -1, 2)):
+                k = k + jnp.where(i >= later, more, 0)
 
             def landed(n, unused):
-                forward_c(k * per + n).wait_recv()
-                forward_xc(k * per + n).wait_recv()
+                ref = rows.at[k, c, n, x]
+                for way in range(2):
+                    remote(ref, ref, c_send.at[k * per + n, way], c_recv.at[k * per + n, way], mate).wait_recv()
                 return unused
 
             lax.fori_loop(0, per, landed, 0)
             experts(k)
-            send_p(k).start()
+
+        @pl.when(i == unit)
+        def _():
+            own_rows(groups[1][: per // 2])
+
+        @pl.when(i == 2 * unit)
+        def _():
+            own_rows(groups[1][per // 2 :])
+            cross_rows(groups[1][: per // 2])
+
+        @pl.when(i == 3 * unit)
+        def _():
+            first_sum(2)
+
+        @pl.when(i == 5 * unit)
+        def _():
+            first_sum(0)
+            last_sum(2)
+
+        @pl.when(i == 6 * unit)
+        def _():
+            first_sum(3)
+            first_sum(1)
+
+        @pl.when(i == 7 * unit)
+        def _():
+            last_sum(0)
+            last_sum(3)
+
+        @pl.when(i == 8 * unit)
+        def _():
+            last_sum(1)
 
         return unused
 
-    lax.fori_loop(0, first_chunk + (chunks - 1) * per + 3, step, 0)
+    lax.fori_loop(0, 8 * unit + 1, step, 0)
+    cross_a().wait_recv()
+    out_a_ref[...] = (
+        part_a[c, x].astype(jnp.float32) + got_a[x].astype(jnp.float32) + sum_in_a[...].astype(jnp.float32)
+    ).astype(jnp.bfloat16)
 
     back_in[0] = back_out[0]
 
@@ -378,55 +445,64 @@
         return unused
 
     lax.fori_loop(1, ep, returned, 0)
-    spots = lax.broadcasted_iota(jnp.int32, (tok, ep * cap), 1)
-    share = jnp.zeros((tok, ep * cap), jnp.float32)
-    for choice in range(slot_cols_ref.shape[1]):
-        share = share + jnp.where(spots == slot_cols_ref[:, choice : choice + 1], mix_ref[:, choice : choice + 1], 0.0)
-    high = share.astype(jnp.bfloat16)
-    rest = share - high.astype(jnp.float32)
-    low = rest.astype(jnp.bfloat16)
+    for d in range(ep):
+        picks = routes_ref[...] == xor(me, d, ep)
+        weight = jnp.sum(jnp.where(picks, mix_ref[...], 0.0), axis=0, keepdims=True)
+        share = hit[d].astype(jnp.float32) * weight
+        high = share.astype(bf16)
+        share_high[d] = high
+        share_low[d] = (share - high.astype(jnp.float32)).astype(bf16)
+    over_rows = (((0,), (0,)), ((), ()))
     for lane in range(0, width, strip):
         piece = back_in[:, :, lane : lane + strip].reshape(ep * cap, strip)
-        out_b_ref[:, lane : lane + strip] = (
-            jnp.dot(high, piece, preferred_element_type=jnp.float32)
-            + jnp.dot(low, piece, preferred_element_type=jnp.float32)
-        ).astype(jnp.bfloat16)
+        total = lax.dot_general(
+            share_high[...].reshape(ep * cap, tok), piece, over_rows, preferred_element_type=jnp.float32
+        ) + lax.dot_general(
+            share_low[...].reshape(ep * cap, tok), piece, over_rows, preferred_element_type=jnp.float32
+        )
+        out_b_ref[:, lane : lane + strip] = total.astype(bf16)
 
     @pl.when(odd == 0)
     def _():
         for copy in own_kv(pair, kv_psend.at[me]):
             copy.wait_send()
 
-    def left_up(step, unused):
-        for copy in own_kv(me + 2 * step, kv_zsend.at[step]):
+    @pl.when(up < upper - 1)
+    def _():
+        for copy in own_kv(me + 2, kv_zsend.at[me]):
             copy.wait_send()
+
+    def left_pair(step, unused):
+        source = me - 2 * step
+        for copy in passed_kv(source, pair, kv_psend):
+            copy.wait_send()
+
+        @pl.when(up < upper - 1)
+        def _():
+            for copy in passed_kv(source, me + 2, kv_zsend):
+                copy.wait_send()
+
         return unused
 
-    lax.fori_loop(1, upper - up, left_up, 0)
-
-    def left_pair(step, unused):
-        for copy in passed_kv(me - 2 * step, pair):
-            copy.wait_send()
-        return unused
-
     lax.fori_loop(1, up + 1, left_pair, 0)
 
-    def left_rows(d, unused):
-        @pl.when(d > 0)
-        def _():
+    for d in range(ep):
+        if d > 0:
             dispatch(d).wait_send()
-            send_back(d // per, d % per).wait_send()
-
+            send_back(d).wait_send()
         forward_x(d).wait_send()
         forward_c(d).wait_send()
         forward_xc(d).wait_send()
-        return unused
-
-    lax.fori_loop(0, ep, left_rows, 0)
 
     def left_sums(k, unused):
-        send_p(k).wait_send()
-        cross_p(k).wait_send()
+        for j in range(width // strip):
+            send_p(k, j).wait_send()
+
+        def left_cross(n, unused):
+            cross_p(k, n).wait_send()
+            return unused
+
+        lax.fori_loop(0, per, left_cross, 0)
         return unused
 
     lax.fori_loop(0, chunks, left_sums, 0)
@@ -450,7 +526,6 @@
     down_weight,
 ):
     ep, tp = lax.axis_size("ep"), lax.axis_size("tp")
-    me = lax.axis_index("ep")
     block = key_rows.shape[0]
     kv_local = key_rows.shape[1] // HD
     heads = query_rows.shape[1] // HD
@@ -462,11 +537,6 @@
     chunks = 4
     per = ep // chunks
     across = tp // CORES
-    flat = routes.reshape(-1)
-    order = jnp.arange(flat.shape[0])
-    rank = jnp.sum((flat[:, None] == flat[None, :]) & (order[None, :] < order[:, None]), axis=1, dtype=jnp.int32)
-    slots = ((flat ^ me) * cap + rank).reshape(tok, top)
-    bias = jnp.pad(key_bias.T, ((0, 16 - kv_local), (0, 0)))
     half = 128
     tiles = hidden_width // half
     vmem = pl.BlockSpec(memory_space=pltpu.VMEM)
@@ -480,17 +550,20 @@
             jax.ShapeDtypeStruct((own_a, width), bf16),
             jax.ShapeDtypeStruct((tok, width), bf16),
         ),
-        in_specs=[vmem] * 4 + [pl.BlockSpec(memory_space=pltpu.SMEM)] + [vmem] * 5 + [hbm] * 4,
+        in_specs=[vmem] * 4 + [pl.BlockSpec(memory_space=pltpu.SMEM)] + [vmem] * 4 + [hbm] * 4,
         out_specs=(vmem, vmem),
         scratch_shapes=[
             pltpu.VMEM((heads, block, wide), bf16),
             pltpu.VMEM((ep, block, wide), bf16),
             pltpu.VMEM((ep, block, wide), bf16),
-            pltpu.VMEM((ep, 16, block), bf16),
+            pltpu.VMEM((ep, kv_local, block), bf16),
             pltpu.VMEM((heads, block, wide), f32),
             pltpu.VMEM((heads, block, 1), f32),
             pltpu.VMEM((block, heads * HD), bf16),
             pltpu.VMEM((block, block), bf16),
+            pltpu.VMEM((ep, cap, tok), bf16),
+            pltpu.VMEM((ep, cap, tok), bf16),
+            pltpu.VMEM((ep, cap, tok), bf16),
             pltpu.VMEM((ep, cap, width), bf16),
             pltpu.VMEM((chunks, CORES, per, across, cap, width), bf16),
             pltpu.VMEM((CORES * per * across * cap, hidden_width), bf16),
@@ -508,11 +581,11 @@
             pltpu.VMEM((hidden_width, width), bf16),
             pltpu.VMEM((heads * HD, width), bf16),
             dma((2 * tiles + 2,)),
-            dma((ep // 2, 3)),
+            dma((ep, 3)),
             dma((ep, 3)),
             dma((ep, 3)),
             dma((ep,)), dma((ep,)), dma((ep,)), dma((ep,)), dma((ep, 2)), dma((ep, 2)),
-            dma((chunks,)), dma((chunks,)), dma((chunks,)), dma((chunks,)), dma((ep,)), dma((ep,)),
+            dma((chunks, width // 512)), dma((chunks, width // 512)), dma((chunks, per)), dma((chunks, per)), dma((ep,)), dma((ep,)),
             dma((2,)), dma((2,)),
         ],
         compiler_params=pltpu.CompilerParams(
@@ -520,8 +593,8 @@
         ),
         name="step",
     )(
-        query_rows, key_rows, value_rows, bias, head_offset, expert_input, expert_gain[None, :],
-        slots.T, slots, route_weight, out_weight, gate_weight, up_weight, down_weight,
+        query_rows, key_rows, value_rows, key_bias.T, head_offset, expert_input, expert_gain[None, :],
+        routes.T, route_weight.T, out_weight, gate_weight, up_weight, down_weight,
     )
 
 

time: 150 us -> 121 us (0.81)
  the two profiles are of different devices: /device:TPU:15 before, /device:TPU:0 now
where the time goes in v2:
time: 121 us; the launch traced here: 119 us
  Pallas kernels  115 us (95%)
  local copies, waits for them, and re-layouts  3.55 us (3%)
    pallas_call x1, Pallas kernels, body(): pl.pallas_call(functools.partial(step_kernel, ep=ep, chunks=chunks, group...  115 us
    unnamed x2, local copies, waits for them, and re-layouts  3.55 us

profile of v2, /device:TPU:0, one launch (start us, length us, event | category | flops | bytes accessed | tf_op | source)
XLA Modules:
  0.0 119.2 jit_solution(11516143645739367157)
XLA Ops:
  0.6 115.0 %step.1 = (bf16[64,2048]{1,0:T(8,128)(2,1)}, bf16[128,2048]{1,0:T(8,128)(2,1)}) custom-call(bf16[256,512]{1,0:T(8,128)(2,1)} %q_ref.1, bf16[256,128]{1,0:T(8,128)(2,1)} %k_ref.1, bf16[256,128]{1,0:T(8,128)(2,1)} %v_ref.1, bf16[2,256]{1,0:T(2,128)(2,1)} %bitcast.5, f32[8]{0:T(128)} %offset_ref.1, bf16[128,2048]{1,0:T(8,128)(2,1)} %x_ref.1, ...), custom_call_target="tpu_custom_call" | custom-call | tf_op jit(solution)/shard_map/step/pallas_call | solution.py:547
  115.6 1.7 %copy.17 = bf16[64,2048]{1,0:T(8,128)(2,1)} copy(bf16[64,2048]{1,0:T(8,128)(2,1)} %get-tuple-element.4) | data formatting | bytes 524288
  117.3 1.9 %copy.18 = bf16[128,2048]{1,0:T(8,128)(2,1)} copy(bf16[128,2048]{1,0:T(8,128)(2,1)} %get-tuple-element.5) | data formatting | bytes 1048576

commit v3 on v2

--- a/solution.py
+++ b/solution.py
@@ -195,10 +195,7 @@
             if keep is not None:
                 leave = jnp.where(keep, leave, 0.0)
             high = leave.astype(jnp.bfloat16)
-            low = (leave - high.astype(jnp.float32)).astype(jnp.bfloat16)
-            after = jnp.dot(high, tri[...], preferred_element_type=jnp.float32) + jnp.dot(
-                low, tri[...], preferred_element_type=jnp.float32
-            )
+            after = jnp.dot(high, tri[...], preferred_element_type=jnp.float32)
             before = carry[head]
             weights = jnp.exp2(log_take - after - before)
             if keep is not None:
@@ -246,7 +243,7 @@
             ).astype(jnp.bfloat16)
             return unused
 
-        lax.fori_loop(0, tiles, gate_up, 0)
+        lax.fori_loop(0, tiles, gate_up, 0, unroll=True)
 
         def down(j, unused):
             lanes = pl.ds(pl.multiple_of(j * strip, strip), strip)
@@ -255,7 +252,7 @@
             send_p(k, j).start()
             return unused
 
-        lax.fori_loop(0, width // strip, down, 0)
+        lax.fori_loop(0, width // strip, down, 0, unroll=True)
 
     def send_p(k, j):
         lanes = pl.ds(pl.multiple_of(j * strip, strip), strip)
@@ -305,7 +302,21 @@
             if d > 0:
                 send_back(d).start()
 
-    expert_steps = (unit, 3 * unit, 4 * unit, 6 * unit)
+    expert_steps = (unit, 3 * unit, 4 * unit, 5 * unit)
+
+    def tile_at(i):
+        return i
+
+    def hook(j):
+        source = me - 2 * j
+        wait_kv(source)
+        for copy in passed_kv(source, pair, kv_psend):
+            copy.start()
+
+        @pl.when(up < upper - 1)
+        def _():
+            for copy in passed_kv(source, me + 2, kv_zsend):
+                copy.start()
 
     def step(i, unused):
         @pl.when(i == 2 * unit)
@@ -315,40 +326,41 @@
         @pl.when(i == 4 * unit)
         def _():
             own_rows(groups[3])
+            first_sum(2)
 
         @pl.when(i == 0)
         def _():
             tile(k_ref, v_ref, bias_ref, place < key_ids)
 
-        @pl.when((i > 0) & (i <= me))
-        def _():
-            source = me - i
-
-            @pl.when(i % 2 == 1)
+        @pl.when(i == unit)
+        def _():
+            for d in groups[3]:
+                dispatch(d).start()
+
+        def earlier_tile(n, unused):
+            source = me - n
+
+            @pl.when(n % 2 == 1)
             def _():
                 wait_kv(source)
 
             tile(kbuf.at[source], vbuf.at[source], bbuf.at[source], None)
-
-        @pl.when((i % 2 == 0) & (i + 2 <= me))
-        def _():
-            source = me - i - 2
-            wait_kv(source)
-            for copy in passed_kv(source, pair, kv_psend):
-                copy.start()
-
-            @pl.when(up < upper - 1)
-            def _():
-                for copy in passed_kv(source, me + 2, kv_zsend):
-                    copy.start()
-
-        @pl.when(i == me)
+            return unused
+
+        start, stop = tile_at(i), tile_at(i + 1)
+        lax.fori_loop(jnp.where(i == 0, 1, start), jnp.minimum(stop, me + 1), earlier_tile, 0)
+
+        @pl.when((i % 2 == 0) & (i // 2 + 1 <= up))
+        def _():
+            hook(i // 2 + 1)
+
+        @pl.when((start <= me) & (me < stop))
         def _():
             wo_copy.wait()
             project()
             send_a().start()
 
-        @pl.when(i == me + 1)
+        @pl.when((i > 0) & (tile_at(i - 1) <= me) & (me < start))
         def _():
             send_a().wait_recv()
             sum_out_a[...] = (
@@ -367,8 +379,6 @@
 
         @pl.when(i == unit)
         def _():
-            for d in groups[3]:
-                dispatch(d).start()
             cross_rows(groups[0])
 
         @pl.when(i == 3 * unit)
@@ -379,7 +389,7 @@
         def _():
             cross_rows(groups[1][per // 2 :])
 
-        @pl.when(i == 6 * unit)
+        @pl.when(i == 5 * unit)
         def _():
             cross_rows(groups[3])
 
@@ -407,28 +417,24 @@
             own_rows(groups[1][per // 2 :])
             cross_rows(groups[1][: per // 2])
 
-        @pl.when(i == 3 * unit)
-        def _():
-            first_sum(2)
-
         @pl.when(i == 5 * unit)
         def _():
+            first_sum(3)
+            last_sum(2)
+
+        @pl.when(i == 6 * unit)
+        def _():
+            first_sum(1)
             first_sum(0)
-            last_sum(2)
-
-        @pl.when(i == 6 * unit)
-        def _():
-            first_sum(3)
-            first_sum(1)
+            last_sum(3)
 
         @pl.when(i == 7 * unit)
         def _():
+            last_sum(1)
+
+        @pl.when(i == 8 * unit)
+        def _():
             last_sum(0)
-            last_sum(3)
-
-        @pl.when(i == 8 * unit)
-        def _():
-            last_sum(1)
 
         return unused
 

time: 121 us -> 116 us (0.959)
  Pallas kernels: 115 us -> 111 us
    pallas_call x1, Pallas kernels: 115 us -> 111 us  [body(): pl.pallas_call(functools.partial(step_kernel, ep=ep, chunks=chunks, group...]
where the time goes in v3:
time: 116 us; the launch traced here: 115 us
  Pallas kernels  111 us (96%)
  local copies, waits for them, and re-layouts  3.55 us (3%)
    pallas_call x1, Pallas kernels, body(): pl.pallas_call(functools.partial(step_kernel, ep=ep, chunks=chunks, group...  111 us
    unnamed x2, local copies, waits for them, and re-layouts  3.55 us

profile of v3, /device:TPU:0, one launch (start us, length us, event | category | flops | bytes accessed | tf_op | source)
XLA Modules:
  0.0 114.9 jit_solution(8065254320304837481)
XLA Ops:
  0.6 110.7 %step.1 = (bf16[64,2048]{1,0:T(8,128)(2,1)}, bf16[128,2048]{1,0:T(8,128)(2,1)}) custom-call(bf16[256,512]{1,0:T(8,128)(2,1)} %q_ref.1, bf16[256,128]{1,0:T(8,128)(2,1)} %k_ref.1, bf16[256,128]{1,0:T(8,128)(2,1)} %v_ref.1, bf16[2,256]{1,0:T(2,128)(2,1)} %bitcast.5, f32[8]{0:T(128)} %offset_ref.1, bf16[128,2048]{1,0:T(8,128)(2,1)} %x_ref.1, ...), custom_call_target="tpu_custom_call" | custom-call | tf_op jit(solution)/shard_map/step/pallas_call | solution.py:553
  111.4 1.7 %copy.17 = bf16[64,2048]{1,0:T(8,128)(2,1)} copy(bf16[64,2048]{1,0:T(8,128)(2,1)} %get-tuple-element.4) | data formatting | bytes 524288
  113.0 1.9 %copy.18 = bf16[128,2048]{1,0:T(8,128)(2,1)} copy(bf16[128,2048]{1,0:T(8,128)(2,1)} %get-tuple-element.5) | data formatting | bytes 1048576
